TPU v7x, 256 devices: a whole 4x4x8 slice. The times are simulated.
256 devices in a mesh: sp: 64 (over z, x, core), tp: 4 (over y).
Axes of the slice: x: 4, y: 4, z: 8, core: 2. Of those that a mesh axis runs over, the one named last changes fastest.
Arguments:
- moe_input: bfloat16 [16384, 2048], P('sp'), may hold values from -6 to 6
- out_cotangent: bfloat16 [16384, 2048], P('sp'), may hold values from -16 to 16
- routes: int32 [16384, 2], P('sp'), may hold values from 0 to 63, all different within a row; in each aligned block of 256 rows (0 to 255, 256 to 511, ...) at most 12 rows name the same one
- group_weight: float32 [16384], P('sp'), may hold values from 0.5 to 1
- inner_weight: float32 [16384, 2], P('sp'), may hold values from 0.3 to 1
- gate_weight: bfloat16 [64, 2048, 1024], P('sp', None, 'tp'), may hold values from -0.125 to 0.125
- up_weight: bfloat16 [64, 2048, 1024], P('sp', None, 'tp'), may hold values from -0.125 to 0.125
- down_weight: bfloat16 [64, 1024, 2048], P('sp', 'tp'), may hold values from -0.1875 to 0.1875
- value_in: bfloat16 [16384, 1024], P('sp', 'tp'), may hold values from -6 to 6
- gate_in: bfloat16 [16384, 1024], P('sp', 'tp'), may hold values from -6 to 6
- conv_taps: bfloat16 [31, 1024], P(None, 'tp'), may hold values from -1 to 1
- norm_hat: bfloat16 [16384, 1024], P('sp', 'tp'), may hold values from -6 to 6
- norm_rstd: float32 [16384], P('sp'), may hold values from 0.3 to 3
- norm_gain: float32 [1024], P('tp'), may hold values from 0.1 to 1.9
- out_proj: bfloat16 [2048, 1024], P(None, 'tp'), may hold values from -0.1875 to 0.1875
Outputs:
- gate_grad: bfloat16 [64, 2048, 1024], P('sp', None, 'tp')
- up_grad: bfloat16 [64, 2048, 1024], P('sp', None, 'tp')
- down_grad: bfloat16 [64, 1024, 2048], P('sp', 'tp')
- proj_grad: float32 [2048, 1024], P('sp', 'tp')
- value_grad: bfloat16 [16384, 1024], P('sp', 'tp')
- gate_in_grad: bfloat16 [16384, 1024], P('sp', 'tp')
Inputs may be any that keep to these rules, and one draw needn't show every extreme that they name: In the rows of one device (aligned blocks of 256 tokens) no expert is named by more than 12 routes, and in every draw some expert is named by exactly 12 in some block; a token's two experts differ.
All inputs are finite; a program needn't handle non-finite values.
Results may differ from a plain program's by a relative error of at most 0.009.
Values may be sent and summed in bfloat16 or wider, within the bound.
No kernel may reach another device: no remote copies, remote signals or barrier semaphores. Data moves between devices by JAX's collectives and lax.ppermute only.
A program may use at most 128 MiB of HBM per device.

v0:
```python
import jax
import jax.numpy as jnp
from jax import lax
from jax.sharding import PartitionSpec as P


def in_one_piece(arrays, axis, split_dim, concat_dim, along):
    ends, at = ([], 0)
    for a in arrays[:-1]:
        at += a.shape[along]
        ends.append(at)
    both = jnp.concatenate(arrays, axis=along)
    return tuple(
        jnp.split(
            lax.all_to_all(both, axis, split_axis=split_dim, concat_axis=concat_dim, tiled=True),
            ends,
            axis=along,
        )
    )


def split_up(array, dim, count):
    lengths = array.shape
    pieces = array.reshape(*lengths[:dim], count, lengths[dim] // count, *lengths[dim + 1 :])
    return jnp.moveaxis(pieces, dim, 0)


def sum_at_owner(array, axis, dim):
    count = lax.axis_size(axis)
    pieces = lax.all_to_all(split_up(array, dim, count), axis, 0, 0, tiled=True)
    return jnp.sum(pieces.astype(jnp.float32), axis=0)


def in_order(pieces, dim):
    pieces = jnp.moveaxis(pieces, 0, dim)
    lengths = pieces.shape
    return pieces.reshape(*lengths[:dim], lengths[dim] * lengths[dim + 1], *lengths[dim + 2 :])


def sent_to_all(array, axis):
    count = lax.axis_size(axis)
    return lax.all_to_all(
        jnp.broadcast_to(array[None], (count, *array.shape)), axis, 0, 0, tiled=True
    )


def gathered_copies(array, axis, dim):
    return in_order(sent_to_all(array, axis), dim)


def summed_on_arrival(array, axis, dim):
    pieces = split_up(array, dim, lax.axis_size(axis))
    arrived = lax.all_to_all(pieces, axis, split_axis=0, concat_axis=0, tiled=True)
    return arrived.sum(axis=0)


def shifted(block, axis, distance):
    devices = range(lax.axis_size(axis))
    route = [(i - distance, i) for i in devices if i - distance in devices]
    return lax.ppermute(block, axis, route)


def silu_slope(logits, squashed):
    return squashed * (1.0 + logits * (1.0 - squashed))


def on_device(
    moe_input,
    out_cotangent,
    routes,
    group_weight,
    inner_weight,
    gate_weight,
    up_weight,
    down_weight,
    value_in,
    gate_in,
    conv_taps,
    norm_hat,
    norm_rstd,
    norm_gain,
    out_proj,
):
    tok_rows, model_width = moe_input.shape
    local_experts = gate_weight.shape[0]
    sp_count = lax.axis_size("sp")
    tp_count = lax.axis_size("tp")
    all_experts = local_experts * sp_count
    capacity = 3 * tok_rows // all_experts
    col_width = model_width // tp_count
    col_start = lax.axis_index("tp") * col_width
    route_count = 2 * tok_rows
    routes_flat = routes.reshape(route_count)
    one_hot = (routes_flat[:, None] == jnp.arange(all_experts, dtype=jnp.int32)[None, :]).astype(
        jnp.int32
    )
    slot_rank = jnp.sum(one_hot * (jnp.cumsum(one_hot, axis=0) - one_hot), axis=1)
    slot_index = routes_flat * capacity + slot_rank
    slot_owner = (
        jnp.full((all_experts * capacity,), route_count, jnp.int32)
        .at[slot_index]
        .set(jnp.arange(route_count, dtype=jnp.int32))
    )
    route_weight = (group_weight[:, None] * inner_weight).reshape(route_count)
    slot_weight = jnp.concatenate([route_weight, jnp.zeros((1,), jnp.float32)])[slot_owner]
    slot_token = slot_owner // 2
    grad_cols = lax.dynamic_slice_in_dim(out_cotangent, col_start, col_width, 1)
    input_cols = lax.dynamic_slice_in_dim(moe_input, col_start, col_width, 1)
    zero_row = jnp.zeros((1, grad_cols.shape[1]), grad_cols.dtype)
    padded_grad = jnp.concatenate([grad_cols, zero_row])[slot_token]
    padded_input = jnp.concatenate([input_cols, zero_row])[slot_token]
    scaled = (slot_weight[:, None] * padded_grad.astype(jnp.float32)).astype(jnp.bfloat16)
    slot_shape = (sp_count, local_experts * capacity, grad_cols.shape[1])
    arrived = in_one_piece(
        (scaled.reshape(slot_shape), padded_input.reshape(slot_shape)), "sp", 0, 0, 1
    )
    slot_grad, slot_input = (
        lax.all_gather(arrived[0], "tp", axis=2, tiled=True),
        lax.all_gather(arrived[1], "tp", axis=2, tiled=True),
    )

    def by_expert(slot_rows):
        return (
            slot_rows.reshape(sp_count, local_experts, capacity, model_width)
            .transpose(1, 0, 2, 3)
            .reshape(local_experts, sp_count * capacity, model_width)
        )

    expert_grad = by_expert(slot_grad)
    expert_input = by_expert(slot_input)
    gate_pre = jnp.einsum(
        "emd,edf->emf", expert_input, gate_weight, preferred_element_type=jnp.float32
    )
    up_pre = jnp.einsum("emd,edf->emf", expert_input, up_weight, preferred_element_type=jnp.float32)
    gate_sigma = jax.nn.sigmoid(gate_pre)
    hidden_act = (gate_pre * gate_sigma * up_pre).astype(jnp.bfloat16)
    act_grad = jnp.einsum(
        "emd,efd->emf", expert_grad, down_weight, preferred_element_type=jnp.float32
    )
    gate_delta = (act_grad * up_pre * silu_slope(gate_pre, gate_sigma)).astype(jnp.bfloat16)
    up_delta = (act_grad * gate_pre * gate_sigma).astype(jnp.bfloat16)
    down_grad = jnp.einsum(
        "emf,emd->efd", hidden_act, expert_grad, preferred_element_type=jnp.float32
    ).astype(jnp.bfloat16)
    gate_grad = jnp.einsum(
        "emd,emf->edf", expert_input, gate_delta, preferred_element_type=jnp.float32
    ).astype(jnp.bfloat16)
    up_grad = jnp.einsum(
        "emd,emf->edf", expert_input, up_delta, preferred_element_type=jnp.float32
    ).astype(jnp.bfloat16)
    partial_value = jnp.einsum(
        "emf,edf->emd", gate_delta, gate_weight, preferred_element_type=jnp.float32
    )
    partial_value = partial_value + jnp.einsum(
        "emf,edf->emd", up_delta, up_weight, preferred_element_type=jnp.float32
    )
    summed = sum_at_owner(
        partial_value.astype(jnp.bfloat16).astype(jnp.float32).astype(jnp.bfloat16), "tp", 2
    )
    returned = summed.astype(jnp.bfloat16).reshape(local_experts, sp_count, capacity, col_width)
    returned = returned.transpose(1, 0, 2, 3).reshape(sp_count, local_experts * capacity, col_width)
    arrived_back = lax.all_to_all(returned, "sp", split_axis=0, concat_axis=0, tiled=True)
    route_grad = arrived_back.reshape(all_experts * capacity, col_width)[slot_index].astype(
        jnp.float32
    )
    mixed_cols = jnp.sum(route_grad.reshape(tok_rows, 2, col_width), axis=1)
    own_cols = lax.dynamic_slice_in_dim(out_cotangent, col_start, col_width, 1).astype(jnp.float32)
    mixer_part = (own_cols + mixed_cols).astype(jnp.bfloat16)
    mixer_grad = gathered_copies(mixer_part, "tp", 1)
    normed = norm_hat.astype(jnp.float32) * norm_gain[None, :]
    norm_sigma = jax.nn.sigmoid(normed)
    mixer_act = (normed * norm_sigma).astype(jnp.bfloat16)
    proj_grad = summed_on_arrival(
        jnp.einsum("tc,tk->ck", mixer_grad, mixer_act, preferred_element_type=jnp.float32), "sp", 0
    )
    silu_grad = jnp.dot(mixer_grad, out_proj, preferred_element_type=jnp.float32)
    hat_grad = silu_grad * silu_slope(normed, norm_sigma) * norm_gain[None, :]
    norm_values = norm_hat.astype(jnp.float32)
    grad_sum, grad_dot = lax.psum(
        (jnp.sum(hat_grad, axis=1), jnp.sum(hat_grad * norm_values, axis=1)), "tp"
    )
    channels = norm_values.shape[1] * tp_count
    conv_grad = norm_rstd[:, None] * (
        hat_grad - grad_sum[:, None] / channels - norm_values * (grad_dot[:, None] / channels)
    )
    tap_count = conv_taps.shape[0]
    incoming = shifted(conv_grad[: tap_count - 1], "sp", -1)
    extended = jnp.concatenate([conv_grad, incoming], axis=0)
    tap_values = conv_taps.astype(jnp.float32)
    glu_grad = jnp.zeros_like(conv_grad)
    for offset in range(tap_count):
        lower = tap_count - 1 - offset
        glu_grad = glu_grad + tap_values[offset][None, :] * extended[lower : lower + tok_rows]
    input_sigma = jax.nn.sigmoid(gate_in.astype(jnp.float32))
    value_grad = (glu_grad * input_sigma).astype(jnp.bfloat16)
    gate_in_grad = (
        glu_grad * value_in.astype(jnp.float32) * input_sigma * (1.0 - input_sigma)
    ).astype(jnp.bfloat16)
    return (gate_grad, up_grad, down_grad, proj_grad, value_grad, gate_in_grad)


def solution(mesh):
    return jax.shard_map(
        on_device,
        mesh=mesh,
        in_specs=(
            P("sp", None),
            P("sp", None),
            P("sp", None),
            P("sp"),
            P("sp", None),
            P("sp", None, "tp"),
            P("sp", None, "tp"),
            P("sp", "tp", None),
            P("sp", "tp"),
            P("sp", "tp"),
            P(None, "tp"),
            P("sp", "tp"),
            P("sp"),
            P("tp"),
            P(None, "tp"),
        ),
        out_specs=(
            P("sp", None, "tp"),
            P("sp", None, "tp"),
            P("sp", "tp", None),
            P("sp", "tp"),
            P("sp", "tp"),
            P("sp", "tp"),
        ),
        check_vma=False,
    )
```

profile of v0, /device:TPU:2, one launch (start us, length us, event | category | flops | bytes accessed | tf_op | source)
XLA Modules:
  0.0 374.2 jit_solution(73980024878958464)
XLA Ops:
  11.0 2.4 scatter_custom_fusion
  14.6 2.7 gather_fusion.2
  18.5 3.3 gather_fusion.1
  23.4 3.2 gather_fusion
  28.4 51.8 %all_to_all.25 = bf16[64,24,512]{2,1,0:T(8,128)(2,1)S(1)} all-to-all(bf16[64,24,512]{2,1,0:T(8,128)(2,1)S(1)} %pad_maximum_fusion), channel_id=1, replica_groups=mesh['sp'=64,'tp'=4] {'sp'}, dimensions={0} | all-to-all | bytes 3145728 | tf_op jit(solution)/shard_map/all_to_all | solution.py:15
  80.3 1.9 fusion.132
  82.9 46.5 %all-gather.3.cloned.1.call-done = bf16[64,12,2048]{2,1,0:T(8,128)(2,1)} async-done(((bf16[64,12,512]{2,1,0:T(8,128)(2,1)}), bf16[64,12,2048]{2,1,0:T(8,128)(2,1)}) %all-gather.3.cloned.1.call-update) | async-done | bytes 3145744 | tf_op jit(solution)/shard_map/all_gather | solution.py:119
  129.4 6.2 %reshape.170 = bf16[768,2048]{1,0:T(8,128)(2,1)} reshape(bf16[64,12,2048]{2,1,0:T(8,128)(2,1)} %all-gather.3.cloned.1.call-done) | data formatting | bytes 6291456 | tf_op jit(solution)/shard_map/reshape.22
  135.6 3.9 %fusion.6 = f32[768,256]{1,0:T(8,128)} fusion(bf16[768,2048]{1,0:T(8,128)(2,1)} %reshape.170, bf16[1,2048,256]{2,1,0:T(8,128)(2,1)S(1)} %copy-done), kind=kOutput, calls=%fused_computation.48 | convolution fusion | flops 805306368 | bytes 4980736 | tf_op jit(solution)/shard_map/emd,edf->emf/dot_general | solution.py:131
  139.5 2.0 fusion.9
  141.5 41.5 %all-gather.5.cloned.1.call-done = bf16[64,12,2048]{2,1,0:T(8,128)(2,1)} async-done(((bf16[64,12,512]{2,1,0:T(8,128)(2,1)}), bf16[64,12,2048]{2,1,0:T(8,128)(2,1)}) %all-gather.5.cloned.1.call-update) | async-done | bytes 3145744 | tf_op jit(solution)/shard_map/all_gather | solution.py:118
  183.0 6.2 %reshape.171 = bf16[768,2048]{1,0:T(8,128)(2,1)} reshape(bf16[64,12,2048]{2,1,0:T(8,128)(2,1)} %all-gather.5.cloned.1.call-done) | data formatting | bytes 6291456 | tf_op jit(solution)/shard_map/reshape.3
  189.1 3.8 %multiply_convert_fusion.2 = (bf16[768,256]{1,0:T(8,128)(2,1)S(1)}, bf16[768,256]{1,0:T(8,128)(2,1)S(1)}) fusion(f32[768,256]{1,0:T(8,128)} %fusion.6, f32[768,256]{1,0:T(8,128)} %fusion.9, bf16[768,2048]{1,0:T(8,128)(2,1)} %reshape.171, bf16[1,256,2048]{2,1,0:T(8,128)(2,1)} %param.22), kind=kOutput, calls=%fused_computation.56 | convolution fusion | flops 807862272 | bytes 6553600 | tf_op jit(solution)/shard_map/emd,efd->emf/dot_general | solution.py:137
  194.0 2.7 add_convert_fusion
  196.7 4.8 %reshape.175 = bf16[1,768,4,512]{3,2,1,0:T(4,128)(2,1)S(1)} reshape(bf16[768,2048]{1,0:T(8,128)(2,1)} %add_convert_fusion) | data formatting | bytes 6291456 | tf_op jit(solution)/shard_map/reshape | solution.py:24
  202.1 40.5 %all_to_all.26 = bf16[4,1,768,512]{3,2,1,0:T(8,128)(2,1)S(1)} all-to-all(bf16[4,1,768,512]{3,2,1,0:T(8,128)(2,1)S(1)} %bitcast.99), channel_id=1, replica_groups=mesh['sp'=64,'tp'=4] {'tp'}, dimensions={0} | all-to-all | bytes 6291456 | tf_op jit(solution)/shard_map/all_to_all | solution.py:30
  242.6 1.6 reduce_sum.61
  244.2 2.1 reshape_transpose_reshape.2
  246.3 10.5 %all-to-all-start.2 = ((bf16[64,12,512]{2,1,0:T(8,128)(2,1)}), bf16[64,12,512]{2,1,0:T(8,128)(2,1)S(1)}, u32[]{:S(2)}, u32[]{:S(2)}) async-start(bf16[64,12,512]{2,1,0:T(8,128)(2,1)} %reshape_transpose_reshape.2), calls=%async_computation.2 | async-start | bytes 2097152 | tf_op jit(solution)/shard_map/all_to_all | solution.py:162
  256.9 28.8 %all-to-all-done.2 = bf16[64,12,512]{2,1,0:T(8,128)(2,1)S(1)} async-done(((bf16[64,12,512]{2,1,0:T(8,128)(2,1)}), bf16[64,12,512]{2,1,0:T(8,128)(2,1)S(1)}, u32[]{:S(2)}, u32[]{:S(2)}) %all-to-all-start.2) | async-done | bytes 786464 | tf_op jit(solution)/shard_map/all_to_all | solution.py:162
  285.8 2.0 gather_fusion.3
  288.5 1.2 reduce_sum.62
  290.0 16.8 %all_to_all.27 = bf16[4,256,512]{1,2,0:T(8,128)(2,1)S(1)} all-to-all(bf16[4,256,512]{1,2,0:T(8,128)(2,1)S(1)} %broadcast_in_dim.11), channel_id=1, replica_groups=mesh['sp'=64,'tp'=4] {'tp'}, dimensions={0} | all-to-all | bytes 2097152 | tf_op jit(solution)/shard_map/all_to_all | solution.py:42
  306.9 1.8 fusion.116
  308.7 6.6 %all-to-all-start.4 = ((f32[64,32,256]{2,1,0:T(8,128)}), f32[64,32,256]{2,1,0:T(8,128)S(1)}, u32[]{:S(2)}, u32[]{:S(2)}) async-start(f32[64,32,256]{2,1,0:T(8,128)} %fusion.116), calls=%async_computation.4 | async-start | bytes 4194304 | tf_op jit(solution)/shard_map/all_to_all | solution.py:53
  316.7 4.0 %fusion = bf16[1,2048,256]{2,1,0:T(8,128)(2,1)} fusion(bf16[768,2048]{1,0:T(8,128)(2,1)} %reshape.170, bf16[768,256]{1,0:T(8,128)(2,1)S(1)} %copy-done.6), kind=kOutput, calls=%fused_computation.39 | convolution fusion | flops 805830656 | bytes 4587520 | tf_op jit(solution)/shard_map/emd,emf->edf/dot_general | solution.py:145
  320.8 2.1 fusion.2
  323.5 8.9 %all-reduce.2 = (f32[256]{0:T(256)S(1)}, f32[256]{0:T(256)S(1)}) all-reduce(f32[256]{0:T(256)S(1)} %get-tuple-element.7, f32[256]{0:T(256)S(1)} %get-tuple-element.6), channel_id=1, replica_groups=mesh['sp'=64,'tp'=4] {'tp'}, use_global_device_ids=true, to_apply=%region_10.11 | all-reduce | flops 512 | bytes 4096 | tf_op jit(solution)/shard_map/psum | solution.py:179
  332.9 1.9 collective-permute-start
  334.8 4.0 %fusion.1 = bf16[1,2048,256]{2,1,0:T(8,128)(2,1)} fusion(bf16[768,2048]{1,0:T(8,128)(2,1)} %reshape.170, bf16[768,256]{1,0:T(8,128)(2,1)} %copy-done.11), kind=kOutput, calls=%fused_computation.40 | convolution fusion | flops 805830656 | bytes 4587520 | tf_op jit(solution)/shard_map/emd,emf->edf/dot_general | solution.py:148
  339.2 2.1 multiply_convert_fusion.5
  342.0 24.6 %all-to-all-done.4 = f32[64,32,256]{2,1,0:T(8,128)S(1)} async-done(((f32[64,32,256]{2,1,0:T(8,128)}), f32[64,32,256]{2,1,0:T(8,128)S(1)}, u32[]{:S(2)}, u32[]{:S(2)}) %all-to-all-start.4) | async-done | bytes 2097184 | tf_op jit(solution)/shard_map/all_to_all | solution.py:53
  (156 shorter events, 16.7 us)
Async XLA Ops:
  7.2 128.4 %copy-start = (bf16[1,2048,256]{2,1,0:T(8,128)(2,1)S(1)}, bf16[1,2048,256]{2,1,0:T(8,128)(2,1)}, u32[]{:S(2)}) copy-start(bf16[1,2048,256]{2,1,0:T(8,128)(2,1)} %param.20) | copy-start | bytes 3145732
  7.2 122.2 %all-gather.3.cloned.1.call-start = ((), (), s32[]{:S(2)}) async-start(), calls=%async_computation.5 | async-start | bytes 5242880 | tf_op jit(solution)/shard_map/all_gather | solution.py:119
  82.1 100.8 %all-gather.5.cloned.1.call-start = ((), (), s32[]{:S(2)}) async-start(), calls=%async_computation.6 | async-start | bytes 5242880 | tf_op jit(solution)/shard_map/all_gather | solution.py:118
  246.3 39.3 %all-to-all-start.2 = ((bf16[64,12,512]{2,1,0:T(8,128)(2,1)}), bf16[64,12,512]{2,1,0:T(8,128)(2,1)S(1)}, u32[]{:S(2)}, u32[]{:S(2)}) async-start(bf16[64,12,512]{2,1,0:T(8,128)(2,1)} %reshape_transpose_reshape.2), calls=%async_computation.2 | async-start | bytes 2097152 | tf_op jit(solution)/shard_map/all_to_all | solution.py:162
  288.4 18.4 %copy-start.8 = (bf16[256,256]{1,0:T(8,128)(2,1)S(1)}, bf16[256,256]{1,0:T(8,128)(2,1)}, u32[]{:S(2)}) copy-start(bf16[256,256]{1,0:T(8,128)(2,1)} %param.26) | copy-start | bytes 393220
  288.5 18.4 %copy-start.46 = (f32[256]{0:T(256)S(1)}, f32[256]{0:T(256)}, u32[]{:S(2)}) copy-start(f32[256]{0:T(256)} %param.28) | copy-start | bytes 3076
  306.8 8.5 %copy-start.13 = (bf16[31,256]{1,0:T(8,128)(2,1)S(1)}, bf16[31,256]{1,0:T(8,128)(2,1)}, u32[]{:S(2)}) copy-start(bf16[31,256]{1,0:T(8,128)(2,1)} %param.25) | copy-start | bytes 47620
  306.9 9.8 %copy-start.6 = (bf16[768,256]{1,0:T(8,128)(2,1)S(1)}, bf16[768,256]{1,0:T(8,128)(2,1)}, u32[]{:S(2)}) copy-start(bf16[768,256]{1,0:T(8,128)(2,1)} %copy-done.5) | copy-start | bytes 1179652
  308.7 57.9 %all-to-all-start.4 = ((f32[64,32,256]{2,1,0:T(8,128)}), f32[64,32,256]{2,1,0:T(8,128)S(1)}, u32[]{:S(2)}, u32[]{:S(2)}) async-start(f32[64,32,256]{2,1,0:T(8,128)} %fusion.116), calls=%async_computation.4 | async-start | bytes 4194304 | tf_op jit(solution)/shard_map/all_to_all | solution.py:53
  322.9 9.5 %copy-start.48 = (f32[256]{0:T(256)S(1)}, f32[256]{0:T(256)}, u32[]{:S(2)}) copy-start(f32[256]{0:T(256)} %param.27) | copy-start | bytes 3076
  332.6 6.3 %copy-start.10 = (bf16[256,256]{1,0:T(8,128)(2,1)S(1)}, bf16[256,256]{1,0:T(8,128)(2,1)}, u32[]{:S(2)}) copy-start(bf16[256,256]{1,0:T(8,128)(2,1)} %param.24) | copy-start | bytes 393220
  332.6 6.3 %copy-start.12 = (bf16[256,256]{1,0:T(8,128)(2,1)S(1)}, bf16[256,256]{1,0:T(8,128)(2,1)}, u32[]{:S(2)}) copy-start(bf16[256,256]{1,0:T(8,128)(2,1)} %param.23) | copy-start | bytes 393220
  332.6 6.3 %copy-start.14 = (f32[1,256]{1,0:T(1,128)S(1)}, f32[1,256]{1,0:T(1,128)}, u32[]{:S(2)}) copy-start(f32[1,256]{1,0:T(1,128)} %get-tuple-element.35) | copy-start | bytes 3076
  332.6 6.3 %copy-start.15 = (f32[1,256]{1,0:T(1,128)S(1)}, f32[1,256]{1,0:T(1,128)}, u32[]{:S(2)}) copy-start(f32[1,256]{1,0:T(1,128)} %get-tuple-element.36) | copy-start | bytes 3076
  332.6 6.3 %copy-start.16 = (f32[1,256]{1,0:T(1,128)S(1)}, f32[1,256]{1,0:T(1,128)}, u32[]{:S(2)}) copy-start(f32[1,256]{1,0:T(1,128)} %get-tuple-element.37) | copy-start | bytes 3076
  332.6 6.3 %copy-start.17 = (f32[1,256]{1,0:T(1,128)S(1)}, f32[1,256]{1,0:T(1,128)}, u32[]{:S(2)}) copy-start(f32[1,256]{1,0:T(1,128)} %get-tuple-element.38) | copy-start | bytes 3076
  332.6 6.3 %copy-start.18 = (f32[1,256]{1,0:T(1,128)S(1)}, f32[1,256]{1,0:T(1,128)}, u32[]{:S(2)}) copy-start(f32[1,256]{1,0:T(1,128)} %get-tuple-element.39) | copy-start | bytes 3076
  332.6 6.3 %copy-start.19 = (f32[1,256]{1,0:T(1,128)S(1)}, f32[1,256]{1,0:T(1,128)}, u32[]{:S(2)}) copy-start(f32[1,256]{1,0:T(1,128)} %get-tuple-element.40) | copy-start | bytes 3076
  332.7 6.3 %copy-start.20 = (f32[1,256]{1,0:T(1,128)S(1)}, f32[1,256]{1,0:T(1,128)}, u32[]{:S(2)}) copy-start(f32[1,256]{1,0:T(1,128)} %get-tuple-element.41) | copy-start | bytes 3076
  332.7 6.3 %copy-start.21 = (f32[1,256]{1,0:T(1,128)S(1)}, f32[1,256]{1,0:T(1,128)}, u32[]{:S(2)}) copy-start(f32[1,256]{1,0:T(1,128)} %get-tuple-element.42) | copy-start | bytes 3076
  332.7 6.3 %copy-start.22 = (f32[1,256]{1,0:T(1,128)S(1)}, f32[1,256]{1,0:T(1,128)}, u32[]{:S(2)}) copy-start(f32[1,256]{1,0:T(1,128)} %get-tuple-element.43) | copy-start | bytes 3076
  332.7 6.3 %copy-start.23 = (f32[1,256]{1,0:T(1,128)S(1)}, f32[1,256]{1,0:T(1,128)}, u32[]{:S(2)}) copy-start(f32[1,256]{1,0:T(1,128)} %get-tuple-element.44) | copy-start | bytes 3076
  332.7 6.3 %copy-start.24 = (f32[1,256]{1,0:T(1,128)S(1)}, f32[1,256]{1,0:T(1,128)}, u32[]{:S(2)}) copy-start(f32[1,256]{1,0:T(1,128)} %get-tuple-element.45) | copy-start | bytes 3076
  332.7 6.3 %copy-start.25 = (f32[1,256]{1,0:T(1,128)S(1)}, f32[1,256]{1,0:T(1,128)}, u32[]{:S(2)}) copy-start(f32[1,256]{1,0:T(1,128)} %get-tuple-element.46) | copy-start | bytes 3076
  332.7 6.3 %copy-start.26 = (f32[1,256]{1,0:T(1,128)S(1)}, f32[1,256]{1,0:T(1,128)}, u32[]{:S(2)}) copy-start(f32[1,256]{1,0:T(1,128)} %get-tuple-element.16) | copy-start | bytes 3076
  332.7 6.3 %copy-start.27 = (f32[1,256]{1,0:T(1,128)S(1)}, f32[1,256]{1,0:T(1,128)}, u32[]{:S(2)}) copy-start(f32[1,256]{1,0:T(1,128)} %get-tuple-element.17) | copy-start | bytes 3076
  332.7 6.3 %copy-start.28 = (f32[1,256]{1,0:T(1,128)S(1)}, f32[1,256]{1,0:T(1,128)}, u32[]{:S(2)}) copy-start(f32[1,256]{1,0:T(1,128)} %get-tuple-element.18) | copy-start | bytes 3076
  332.7 6.3 %copy-start.29 = (f32[1,256]{1,0:T(1,128)S(1)}, f32[1,256]{1,0:T(1,128)}, u32[]{:S(2)}) copy-start(f32[1,256]{1,0:T(1,128)} %get-tuple-element.19) | copy-start | bytes 3076
  332.8 6.3 %copy-start.30 = (f32[1,256]{1,0:T(1,128)S(1)}, f32[1,256]{1,0:T(1,128)}, u32[]{:S(2)}) copy-start(f32[1,256]{1,0:T(1,128)} %get-tuple-element.20) | copy-start | bytes 3076
  332.8 6.3 %copy-start.31 = (f32[1,256]{1,0:T(1,128)S(1)}, f32[1,256]{1,0:T(1,128)}, u32[]{:S(2)}) copy-start(f32[1,256]{1,0:T(1,128)} %get-tuple-element.21) | copy-start | bytes 3076
  332.9 6.0 %collective-permute-start = (f32[30,256]{1,0:T(8,128)S(1)}, f32[30,256]{1,0:T(8,128)S(1)}, u32[]{:S(2)}, u32[]{:S(2)}) collective-permute-start(f32[30,256]{1,0:T(8,128)S(1)} %slice.266), channel_id=1, source_target_pairs={{4,0},{8,4},{12,8},{16,12},{20,16},{24,20},{28,24},{32,28},{36,32}... | collective-permute-start | bytes 92168 | tf_op jit(solution)/shard_map/ppermute | solution.py:60
  334.8 32.5 %copy-start.1 = (bf16[1,2048,256]{2,1,0:T(8,128)(2,1)S(1)}, bf16[1,2048,256]{2,1,0:T(8,128)(2,1)}, u32[]{:S(2)}) copy-start(bf16[1,2048,256]{2,1,0:T(8,128)(2,1)} %param.20) | copy-start | bytes 3145732
  (26 other events, 120.8 us)
Sparse Core Ops, SparseCore 0:
  82.3 47.1 all-gather.2
  131.8 51.1 all-gather.4
where the time goes:
time: 375 us; the launch traced here: 374 us
  waiting for transfers between devices  142 us (38%)
  blocking collectives  118 us (31%)
  local copies, waits for them, and re-layouts  44.3 us (12%)
  matrix products  26 us (7%)
  starting transfers between devices  19.4 us (5%)
  between operations  15 us (4%)
  other arithmetic  9.55 us (3%)
    all_to_all x1, blocking collectives, in_one_piece(): lax.all_to_all(both, axis, split_axis=split_dim, concat_axis=concat_dim,...  51.8 us
    all_gather x1, waiting for transfers between devices, on_device(): lax.all_gather(arrived[1], 'tp', axis=2, tiled=True)  46.5 us
    all_gather x1, waiting for transfers between devices, on_device(): lax.all_gather(arrived[0], 'tp', axis=2, tiled=True)  41.5 us
    all_to_all x1, blocking collectives, sum_at_owner(): pieces = lax.all_to_all(split_up(array, dim, count), axis, 0, 0, tiled=True)  40.5 us
    all_to_all x1, waiting for transfers between devices, on_device(): lax.all_to_all(returned, 'sp', split_axis=0, concat_axis=0, tiled=True)  28.8 us
    all_to_all x1, waiting for transfers between devices, summed_on_arrival(): lax.all_to_all(pieces, axis, split_axis=0, concat_axis=0, tiled=True)  24.6 us
    all_to_all x1, blocking collectives, sent_to_all(): lax.all_to_all(jnp.broadcast_to(array[None], (count, *array.shape)), axis...  16.8 us
    another operation x3, local copies, waits for them, and re-layouts  12.3 us
  transfers between devices with their start and end apart: 5, of which 4 were waited for; matrix products, arithmetic and copies ran while one was open for 7% of the time, Pallas kernels for 0%

commit v1 on v0

--- a/solution.py
+++ b/solution.py
@@ -2,6 +2,11 @@
 import jax.numpy as jnp
 from jax import lax
 from jax.sharding import PartitionSpec as P
+
+
+def gathered_along(block, axis, dim):
+    blocks = lax.all_gather(block, axis)
+    return jnp.concatenate(blocks, axis=dim)
 
 
 def in_one_piece(arrays, axis, split_dim, concat_dim, along):
@@ -115,7 +120,7 @@
         (scaled.reshape(slot_shape), padded_input.reshape(slot_shape)), "sp", 0, 0, 1
     )
     slot_grad, slot_input = (
-        lax.all_gather(arrived[0], "tp", axis=2, tiled=True),
+        gathered_along(arrived[0], "tp", 2),
         lax.all_gather(arrived[1], "tp", axis=2, tiled=True),
     )
 

time: 375 us -> 363 us (0.968)
  waiting for transfers between devices: 142 us -> 132 us
    all_gather x1, waiting for transfers between devices: 41.5 us -> 32.9 us  [gathered_along(): blocks = lax.all_gather(block, axis)]
    another operation x3 -> x2, local copies, waits for them, and re-layouts: 12.3 us -> 6.17 us
    all_gather x0 -> x1, local copies, waits for them, and re-layouts: none -> 4.32 us  [gathered_along(): blocks = lax.all_gather(block, axis)]
  transfers between devices with their start and end apart: 5 -> 5, of which waited for: 4 -> 4; matrix products, arithmetic and copies ran while one was open for 7% -> 8% of each run, Pallas kernels for 0% -> 0%
where the time goes in v1:
time: 363 us; the launch traced here: 362 us
  waiting for transfers between devices  132 us (36%)
  blocking collectives  118 us (33%)
  local copies, waits for them, and re-layouts  45.1 us (12%)
  matrix products  23.4 us (6%)
  starting transfers between devices  19.2 us (5%)
  between operations  15.1 us (4%)
  other arithmetic  9.55 us (3%)
    all_to_all x1, blocking collectives, in_one_piece(): lax.all_to_all(both, axis, split_axis=split_dim, concat_axis=concat_dim,...  51.8 us
    all_gather x1, waiting for transfers between devices, on_device(): lax.all_gather(arrived[1], 'tp', axis=2, tiled=True)  45.7 us
    all_to_all x1, blocking collectives, sum_at_owner(): pieces = lax.all_to_all(split_up(array, dim, count), axis, 0, 0, tiled=True)  40.4 us
    all_gather x1, waiting for transfers between devices, gathered_along(): blocks = lax.all_gather(block, axis)  32.9 us
    all_to_all x1, waiting for transfers between devices, on_device(): lax.all_to_all(returned, 'sp', split_axis=0, concat_axis=0, tiled=True)  28.8 us
    all_to_all x1, waiting for transfers between devices, summed_on_arrival(): lax.all_to_all(pieces, axis, split_axis=0, concat_axis=0, tiled=True)  24.6 us
    all_to_all x1, blocking collectives, sent_to_all(): lax.all_to_all(jnp.broadcast_to(array[None], (count, *array.shape)), axis...  16.8 us
    all_to_all x1, starting transfers between devices, on_device(): lax.all_to_all(returned, 'sp', split_axis=0, concat_axis=0, tiled=True)  10.5 us
  transfers between devices with their start and end apart: 5, of which 4 were waited for; matrix products, arithmetic and copies ran while one was open for 8% of the time, Pallas kernels for 0%

profile of v1, /device:TPU:2, one launch (start us, length us, event | category | flops | bytes accessed | tf_op | source)
XLA Modules:
  0.0 362.1 jit_solution(13051979275200827349)
XLA Ops:
  11.0 2.4 scatter_custom_fusion
  14.6 2.7 gather_fusion.2
  18.5 3.3 gather_fusion.1
  23.4 3.2 gather_fusion
  28.4 51.8 %all_to_all.25 = bf16[64,24,512]{2,1,0:T(8,128)(2,1)S(1)} all-to-all(bf16[64,24,512]{2,1,0:T(8,128)(2,1)S(1)} %pad_maximum_fusion), channel_id=1, replica_groups=mesh['sp'=64,'tp'=4] {'sp'}, dimensions={0} | all-to-all | bytes 3145728 | tf_op jit(solution)/shard_map/all_to_all | solution.py:20
  80.3 1.5 fusion.132
  82.0 1.3 copy.34
  83.4 45.7 %all-gather.4.cloned.1.call-done = bf16[64,12,2048]{2,1,0:T(8,128)(2,1)} async-done(((bf16[64,12,512]{2,1,0:T(8,128)(2,1)}), bf16[64,12,2048]{2,1,0:T(8,128)(2,1)}) %all-gather.4.cloned.1.call-update) | async-done | bytes 3145744 | tf_op jit(solution)/shard_map/all_gather | solution.py:124
  129.1 6.2 %reshape.173 = bf16[768,2048]{1,0:T(8,128)(2,1)} reshape(bf16[64,12,2048]{2,1,0:T(8,128)(2,1)} %all-gather.4.cloned.1.call-done) | data formatting | bytes 6291456 | tf_op jit(solution)/shard_map/reshape.23
  135.3 3.9 %fusion.6 = f32[768,256]{1,0:T(8,128)} fusion(bf16[768,2048]{1,0:T(8,128)(2,1)} %reshape.173, bf16[1,2048,256]{2,1,0:T(8,128)(2,1)S(1)} %copy-done), kind=kOutput, calls=%fused_computation.48 | convolution fusion | flops 805306368 | bytes 4980736 | tf_op jit(solution)/shard_map/emd,edf->emf/dot_general | solution.py:136
  139.2 1.9 fusion.9
  141.0 32.9 %all-gather.6.cloned.1.call-done = bf16[256,12,512]{2,0,1:T(8,128)(2,1)} async-done(((bf16[64,12,512]{2,0,1:T(8,128)(2,1)}), bf16[256,12,512]{2,0,1:T(8,128)(2,1)}) %all-gather.6.cloned.1.call-update) | async-done | bytes 3145744 | tf_op jit(solution)/shard_map/all_gather | solution.py:8
  173.9 4.3 %copy.35 = bf16[4,64,12,512]{3,0,2,1:T(4,128)(2,1)S(1)} copy(bf16[4,64,12,512]{3,1,0,2:T(8,128)(2,1)} %bitcast.110) | data formatting | bytes 6291456 | tf_op jit(solution)/shard_map/all_gather | solution.py:8
  182.1 2.8 add_convert_fusion
  185.0 4.8 %reshape.179 = bf16[1,768,4,512]{3,2,1,0:T(4,128)(2,1)S(1)} reshape(bf16[768,2048]{1,0:T(8,128)(2,1)} %add_convert_fusion) | data formatting | bytes 6291456 | tf_op jit(solution)/shard_map/reshape | solution.py:29
  190.4 40.4 %all_to_all.26 = bf16[4,1,768,512]{3,2,1,0:T(8,128)(2,1)S(1)} all-to-all(bf16[4,1,768,512]{3,2,1,0:T(8,128)(2,1)S(1)} %bitcast.105), channel_id=1, replica_groups=mesh['sp'=64,'tp'=4] {'tp'}, dimensions={0} | all-to-all | bytes 6291456 | tf_op jit(solution)/shard_map/all_to_all | solution.py:35
  230.8 1.6 reduce_sum.61
  232.3 2.1 reshape_transpose_reshape.4
  234.4 10.5 %all-to-all-start.2 = ((bf16[64,12,512]{2,1,0:T(8,128)(2,1)}), bf16[64,12,512]{2,1,0:T(8,128)(2,1)S(1)}, u32[]{:S(2)}, u32[]{:S(2)}) async-start(bf16[64,12,512]{2,1,0:T(8,128)(2,1)} %reshape_transpose_reshape.4), calls=%async_computation.2 | async-start | bytes 2097152 | tf_op jit(solution)/shard_map/all_to_all | solution.py:167
  245.0 28.8 %all-to-all-done.2 = bf16[64,12,512]{2,1,0:T(8,128)(2,1)S(1)} async-done(((bf16[64,12,512]{2,1,0:T(8,128)(2,1)}), bf16[64,12,512]{2,1,0:T(8,128)(2,1)S(1)}, u32[]{:S(2)}, u32[]{:S(2)}) %all-to-all-start.2) | async-done | bytes 786464 | tf_op jit(solution)/shard_map/all_to_all | solution.py:167
  273.9 2.0 gather_fusion.3
  276.6 1.2 reduce_sum.62
  278.1 16.8 %all_to_all.27 = bf16[4,256,512]{1,2,0:T(8,128)(2,1)S(1)} all-to-all(bf16[4,256,512]{1,2,0:T(8,128)(2,1)S(1)} %broadcast_in_dim.11), channel_id=1, replica_groups=mesh['sp'=64,'tp'=4] {'tp'}, dimensions={0} | all-to-all | bytes 2097152 | tf_op jit(solution)/shard_map/all_to_all | solution.py:47
  295.0 1.9 fusion.116
  296.8 6.4 %all-to-all-start.4 = ((f32[64,32,256]{2,1,0:T(8,128)}), f32[64,32,256]{2,1,0:T(8,128)S(1)}, u32[]{:S(2)}, u32[]{:S(2)}) async-start(f32[64,32,256]{2,1,0:T(8,128)} %fusion.116), calls=%async_computation.4 | async-start | bytes 4194304 | tf_op jit(solution)/shard_map/all_to_all | solution.py:58
  304.6 4.1 %fusion = bf16[1,2048,256]{2,1,0:T(8,128)(2,1)} fusion(bf16[768,2048]{1,0:T(8,128)(2,1)} %reshape.173, bf16[768,256]{1,0:T(8,128)(2,1)S(1)} %copy-done.7), kind=kOutput, calls=%fused_computation.39 | convolution fusion | flops 805830656 | bytes 4587520 | tf_op jit(solution)/shard_map/emd,emf->edf/dot_general | solution.py:150
  308.7 2.1 fusion.2
  311.4 8.9 %all-reduce.2 = (f32[256]{0:T(256)S(1)}, f32[256]{0:T(256)S(1)}) all-reduce(f32[256]{0:T(256)S(1)} %get-tuple-element.7, f32[256]{0:T(256)S(1)} %get-tuple-element.6), channel_id=1, replica_groups=mesh['sp'=64,'tp'=4] {'tp'}, use_global_device_ids=true, to_apply=%region_10.11 | all-reduce | flops 512 | bytes 4096 | tf_op jit(solution)/shard_map/psum | solution.py:184
  320.8 1.9 collective-permute-start
  322.8 4.0 %fusion.1 = bf16[1,2048,256]{2,1,0:T(8,128)(2,1)} fusion(bf16[768,2048]{1,0:T(8,128)(2,1)} %reshape.173, bf16[768,256]{1,0:T(8,128)(2,1)} %copy-done.12), kind=kOutput, calls=%fused_computation.40 | convolution fusion | flops 805830656 | bytes 4587520 | tf_op jit(solution)/shard_map/emd,emf->edf/dot_general | solution.py:153
  327.1 2.1 multiply_convert_fusion.5
  330.0 24.6 %all-to-all-done.4 = f32[64,32,256]{2,1,0:T(8,128)S(1)} async-done(((f32[64,32,256]{2,1,0:T(8,128)}), f32[64,32,256]{2,1,0:T(8,128)S(1)}, u32[]{:S(2)}, u32[]{:S(2)}) %all-to-all-start.4) | async-done | bytes 2097184 | tf_op jit(solution)/shard_map/all_to_all | solution.py:58
  (166 shorter events, 19.0 us)
Async XLA Ops:
  7.2 128.1 %copy-start = (bf16[1,2048,256]{2,1,0:T(8,128)(2,1)S(1)}, bf16[1,2048,256]{2,1,0:T(8,128)(2,1)}, u32[]{:S(2)}) copy-start(bf16[1,2048,256]{2,1,0:T(8,128)(2,1)} %param.20) | copy-start | bytes 3145732
  7.2 121.9 %all-gather.4.cloned.1.call-start = ((), (), s32[]{:S(2)}) async-start(), calls=%async_computation.5 | async-start | bytes 5242880 | tf_op jit(solution)/shard_map/all_gather | solution.py:124
  81.8 92.1 %all-gather.6.cloned.1.call-start = ((), (), s32[]{:S(2)}) async-start(), calls=%async_computation.6 | async-start | bytes 3932160 | tf_op jit(solution)/shard_map/all_gather | solution.py:8
  234.4 39.3 %all-to-all-start.2 = ((bf16[64,12,512]{2,1,0:T(8,128)(2,1)}), bf16[64,12,512]{2,1,0:T(8,128)(2,1)S(1)}, u32[]{:S(2)}, u32[]{:S(2)}) async-start(bf16[64,12,512]{2,1,0:T(8,128)(2,1)} %reshape_transpose_reshape.4), calls=%async_computation.2 | async-start | bytes 2097152 | tf_op jit(solution)/shard_map/all_to_all | solution.py:167
  276.6 18.4 %copy-start.9 = (bf16[256,256]{1,0:T(8,128)(2,1)S(1)}, bf16[256,256]{1,0:T(8,128)(2,1)}, u32[]{:S(2)}) copy-start(bf16[256,256]{1,0:T(8,128)(2,1)} %param.26) | copy-start | bytes 393220
  276.6 18.4 %copy-start.47 = (f32[256]{0:T(256)S(1)}, f32[256]{0:T(256)}, u32[]{:S(2)}) copy-start(f32[256]{0:T(256)} %param.28) | copy-start | bytes 3076
  295.0 8.3 %copy-start.14 = (bf16[31,256]{1,0:T(8,128)(2,1)S(1)}, bf16[31,256]{1,0:T(8,128)(2,1)}, u32[]{:S(2)}) copy-start(bf16[31,256]{1,0:T(8,128)(2,1)} %param.25) | copy-start | bytes 47620
  295.0 9.6 %copy-start.7 = (bf16[768,256]{1,0:T(8,128)(2,1)S(1)}, bf16[768,256]{1,0:T(8,128)(2,1)}, u32[]{:S(2)}) copy-start(bf16[768,256]{1,0:T(8,128)(2,1)} %copy-done.6) | copy-start | bytes 1179652
  296.8 57.7 %all-to-all-start.4 = ((f32[64,32,256]{2,1,0:T(8,128)}), f32[64,32,256]{2,1,0:T(8,128)S(1)}, u32[]{:S(2)}, u32[]{:S(2)}) async-start(f32[64,32,256]{2,1,0:T(8,128)} %fusion.116), calls=%async_computation.4 | async-start | bytes 4194304 | tf_op jit(solution)/shard_map/all_to_all | solution.py:58
  310.8 9.5 %copy-start.49 = (f32[256]{0:T(256)S(1)}, f32[256]{0:T(256)}, u32[]{:S(2)}) copy-start(f32[256]{0:T(256)} %param.27) | copy-start | bytes 3076
  320.5 6.3 %copy-start.11 = (bf16[256,256]{1,0:T(8,128)(2,1)S(1)}, bf16[256,256]{1,0:T(8,128)(2,1)}, u32[]{:S(2)}) copy-start(bf16[256,256]{1,0:T(8,128)(2,1)} %param.24) | copy-start | bytes 393220
  320.5 6.3 %copy-start.13 = (bf16[256,256]{1,0:T(8,128)(2,1)S(1)}, bf16[256,256]{1,0:T(8,128)(2,1)}, u32[]{:S(2)}) copy-start(bf16[256,256]{1,0:T(8,128)(2,1)} %param.23) | copy-start | bytes 393220
  320.5 6.3 %copy-start.15 = (f32[1,256]{1,0:T(1,128)S(1)}, f32[1,256]{1,0:T(1,128)}, u32[]{:S(2)}) copy-start(f32[1,256]{1,0:T(1,128)} %get-tuple-element.35) | copy-start | bytes 3076
  320.5 6.3 %copy-start.16 = (f32[1,256]{1,0:T(1,128)S(1)}, f32[1,256]{1,0:T(1,128)}, u32[]{:S(2)}) copy-start(f32[1,256]{1,0:T(1,128)} %get-tuple-element.36) | copy-start | bytes 3076
  320.5 6.3 %copy-start.17 = (f32[1,256]{1,0:T(1,128)S(1)}, f32[1,256]{1,0:T(1,128)}, u32[]{:S(2)}) copy-start(f32[1,256]{1,0:T(1,128)} %get-tuple-element.37) | copy-start | bytes 3076
  320.6 6.3 %copy-start.18 = (f32[1,256]{1,0:T(1,128)S(1)}, f32[1,256]{1,0:T(1,128)}, u32[]{:S(2)}) copy-start(f32[1,256]{1,0:T(1,128)} %get-tuple-element.38) | copy-start | bytes 3076
  320.6 6.3 %copy-start.19 = (f32[1,256]{1,0:T(1,128)S(1)}, f32[1,256]{1,0:T(1,128)}, u32[]{:S(2)}) copy-start(f32[1,256]{1,0:T(1,128)} %get-tuple-element.39) | copy-start | bytes 3076
  320.6 6.3 %copy-start.20 = (f32[1,256]{1,0:T(1,128)S(1)}, f32[1,256]{1,0:T(1,128)}, u32[]{:S(2)}) copy-start(f32[1,256]{1,0:T(1,128)} %get-tuple-element.40) | copy-start | bytes 3076
  320.6 6.3 %copy-start.21 = (f32[1,256]{1,0:T(1,128)S(1)}, f32[1,256]{1,0:T(1,128)}, u32[]{:S(2)}) copy-start(f32[1,256]{1,0:T(1,128)} %get-tuple-element.41) | copy-start | bytes 3076
  320.6 6.3 %copy-start.22 = (f32[1,256]{1,0:T(1,128)S(1)}, f32[1,256]{1,0:T(1,128)}, u32[]{:S(2)}) copy-start(f32[1,256]{1,0:T(1,128)} %get-tuple-element.42) | copy-start | bytes 3076
  320.6 6.3 %copy-start.23 = (f32[1,256]{1,0:T(1,128)S(1)}, f32[1,256]{1,0:T(1,128)}, u32[]{:S(2)}) copy-start(f32[1,256]{1,0:T(1,128)} %get-tuple-element.43) | copy-start | bytes 3076
  320.6 6.3 %copy-start.24 = (f32[1,256]{1,0:T(1,128)S(1)}, f32[1,256]{1,0:T(1,128)}, u32[]{:S(2)}) copy-start(f32[1,256]{1,0:T(1,128)} %get-tuple-element.44) | copy-start | bytes 3076
  320.6 6.3 %copy-start.25 = (f32[1,256]{1,0:T(1,128)S(1)}, f32[1,256]{1,0:T(1,128)}, u32[]{:S(2)}) copy-start(f32[1,256]{1,0:T(1,128)} %get-tuple-element.45) | copy-start | bytes 3076
  320.6 6.3 %copy-start.26 = (f32[1,256]{1,0:T(1,128)S(1)}, f32[1,256]{1,0:T(1,128)}, u32[]{:S(2)}) copy-start(f32[1,256]{1,0:T(1,128)} %get-tuple-element.46) | copy-start | bytes 3076
  320.6 6.3 %copy-start.27 = (f32[1,256]{1,0:T(1,128)S(1)}, f32[1,256]{1,0:T(1,128)}, u32[]{:S(2)}) copy-start(f32[1,256]{1,0:T(1,128)} %get-tuple-element.16) | copy-start | bytes 3076
  320.7 6.3 %copy-start.28 = (f32[1,256]{1,0:T(1,128)S(1)}, f32[1,256]{1,0:T(1,128)}, u32[]{:S(2)}) copy-start(f32[1,256]{1,0:T(1,128)} %get-tuple-element.17) | copy-start | bytes 3076
  320.7 6.3 %copy-start.29 = (f32[1,256]{1,0:T(1,128)S(1)}, f32[1,256]{1,0:T(1,128)}, u32[]{:S(2)}) copy-start(f32[1,256]{1,0:T(1,128)} %get-tuple-element.18) | copy-start | bytes 3076
  320.7 6.3 %copy-start.30 = (f32[1,256]{1,0:T(1,128)S(1)}, f32[1,256]{1,0:T(1,128)}, u32[]{:S(2)}) copy-start(f32[1,256]{1,0:T(1,128)} %get-tuple-element.19) | copy-start | bytes 3076
  320.7 6.3 %copy-start.31 = (f32[1,256]{1,0:T(1,128)S(1)}, f32[1,256]{1,0:T(1,128)}, u32[]{:S(2)}) copy-start(f32[1,256]{1,0:T(1,128)} %get-tuple-element.20) | copy-start | bytes 3076
  320.7 6.3 %copy-start.32 = (f32[1,256]{1,0:T(1,128)S(1)}, f32[1,256]{1,0:T(1,128)}, u32[]{:S(2)}) copy-start(f32[1,256]{1,0:T(1,128)} %get-tuple-element.21) | copy-start | bytes 3076
  320.8 6.0 %collective-permute-start = (f32[30,256]{1,0:T(8,128)S(1)}, f32[30,256]{1,0:T(8,128)S(1)}, u32[]{:S(2)}, u32[]{:S(2)}) collective-permute-start(f32[30,256]{1,0:T(8,128)S(1)} %slice.266), channel_id=1, source_target_pairs={{4,0},{8,4},{12,8},{16,12},{20,16},{24,20},{28,24},{32,28},{36,32}... | collective-permute-start | bytes 92168 | tf_op jit(solution)/shard_map/ppermute | solution.py:65
  322.8 32.5 %copy-start.1 = (bf16[1,2048,256]{2,1,0:T(8,128)(2,1)S(1)}, bf16[1,2048,256]{2,1,0:T(8,128)(2,1)}, u32[]{:S(2)}) copy-start(bf16[1,2048,256]{2,1,0:T(8,128)(2,1)} %param.20) | copy-start | bytes 3145732
  (30 other events, 126.9 us)
Sparse Core Ops, SparseCore 0:
  81.9 47.1 all-gather.3
  131.5 42.3 all-gather.5
